TPU v7x, 32 devices: a whole 2x2x4 slice. The times are simulated.
32 devices in a mesh: ep: 8 (over z, core), tp: 4 (over y, x).
Axes of the slice: x: 2, y: 2, z: 4, core: 2. Of those that a mesh axis runs over, the one named last changes fastest.
Arguments:
- pool_input: bfloat16 [2048, 2048], P('ep'), may hold values from -6 to 6
- pool_gain: float32 [2048], replicated, may hold values from 0.1 to 1.9
- pool_weight: bfloat16 [512, 2048], P(None, 'tp'), may hold values from -0.25 to 0.25
- pool_scale: float32 [2048], P('tp'), may hold values from 0.1 to 1.9
- moe_input: bfloat16 [1536, 2048], P('ep'), may hold values from -6 to 6
- moe_gain: float32 [2048], replicated, may hold values from 0.1 to 1.9
- routes: int32 [1536, 2], P('ep'), may hold values from 0 to 7, all different within a row; in each aligned block of 192 rows (0 to 191, 192 to 383, ...) at most 96 rows name the same one
- route_logits: float32 [1536, 2], P('ep'), may hold values from -4 to 4
- gate_weight: bfloat16 [8, 2048, 4096], P('ep', None, 'tp'), may hold values from -0.125 to 0.125
- up_weight: bfloat16 [8, 2048, 4096], P('ep', None, 'tp'), may hold values from -0.125 to 0.125
- down_weight: bfloat16 [8, 2048, 4096], P('ep', None, 'tp'), may hold values from -0.09375 to 0.09375
Outputs:
- pool_out: bfloat16 [2048, 2048], P('ep', 'tp')
- expert_out: bfloat16 [1536, 2048], P('ep', 'tp')
Inputs may be any that keep to these rules, and one draw needn't show every extreme that they name: `routes`: the 2 experts of a token differ. Within the rows of one device (aligned blocks of 192 rows) no expert is named by more than 96 rows, and in every draw some expert is named by exactly 96 rows of some device.
All inputs are finite; a program needn't handle non-finite values.
Results may differ from a plain program's by a relative error of at most 0.017.
Values may be sent and summed in bfloat16 or wider, within the bound.
A program may use at most 64 MiB of HBM per device.

v0:
```python
import functools

import jax
import jax.numpy as jnp
from jax import lax
from jax.experimental import pallas as pl
from jax.experimental.pallas import tpu as pltpu
from jax.sharding import PartitionSpec as P

EPSILON = 1e-06
halo_rows = 16


def expert_kernel(
    sizes,
    tokens_ref,
    gain_ref,
    select_ref,
    blend_ref,
    gate_hbm,
    up_hbm,
    down_hbm,
    pool_in_ref,
    pool_gain_ref,
    pool_weight_ref,
    pool_scale_ref,
    out_ref,
    pool_out_ref,
    normed,
    outgoing,
    sibling_out,
    rows_in,
    parts,
    first_in0,
    first_in1,
    half_sum0,
    half_sum1,
    second_in0,
    second_in1,
    finished,
    returned,
    gate_ref,
    up_ref,
    down_ref,
    pool_own,
    pool_tail,
    pool_halo,
    weight_sem,
    halo_sem,
    go_send,
    go_recv,
    a0_send,
    a0_recv,
    a1_send,
    a1_recv,
    b0_send,
    b0_recv,
    b1_send,
    b1_recv,
    ra0_send,
    ra0_recv,
    ra1_send,
    ra1_recv,
    rb0_send,
    rb0_recv,
    rb1_send,
    rb1_recv,
    back_send,
    back_recv,
):
    experts, ny, nx, slots, columns = sizes
    pairs = experts // 2
    me, shard = lax.axis_index("ep"), lax.axis_index("tp")
    my_pair, my_core = me // 2, me % 2
    my_y, my_x = shard // nx, shard % nx
    bf16, f32 = jnp.bfloat16, jnp.float32
    pending = []

    def device_at(ep, y, x):
        return {"ep": ep, "tp": y * nx + x}

    def copy_to(src, dst, send, recv, target):
        return pltpu.make_async_remote_copy(
            src_ref=src,
            dst_ref=dst,
            send_sem=send,
            recv_sem=recv,
            device_id=target,
            device_id_type=pl.DeviceIdType.MESH,
        )

    def start(*arguments):
        copy = copy_to(*arguments)
        copy.start()
        pending.append(copy)

    def arrive(ref, send, recv):
        copy_to(ref, ref, send, recv, device_at(me, my_y, my_x)).wait_recv()

    weight_copies = [
        pltpu.make_async_copy(source.at[0], target, weight_sem.at[number])
        for number, (source, target) in enumerate(
            ((gate_hbm, gate_ref), (up_hbm, up_ref), (down_hbm, down_ref))
        )
    ]
    for copy in weight_copies:
        copy.start()

    others_x = [lax.rem(my_x + step, nx) for step in range(1, nx)]
    others_y = [lax.rem(my_y + step, ny) for step in range(1, ny)]
    barrier = pltpu.get_barrier_semaphore()
    greeted = [device_at(lax.rem(me + step, experts), my_y, my_x) for step in range(1, experts)]
    greeted += [device_at(me, my_y, x) for x in others_x]
    greeted += [device_at(me, y, my_x) for y in others_y]
    for target in greeted:
        pl.semaphore_signal(
            barrier, inc=1, device_id=target, device_id_type=pl.DeviceIdType.MESH
        )

    values = tokens_ref[...].astype(f32)
    scale = lax.rsqrt(jnp.mean(values * values, axis=-1, keepdims=True) + EPSILON)
    normed[...] = (values * scale * gain_ref[...]).astype(bf16)
    own_columns = pl.ds(pl.multiple_of(shard * columns, columns), columns)
    narrow = normed[:, own_columns]

    def pair_at(step):
        if pairs > 0:
            return lax.rem(my_pair + step, pairs)
        flipped, bit = 0, 1
        while bit < pairs:
            digit = (my_pair // bit) % 2
            flipped = flipped + bit * (1 - digit if step & bit else digit)
            bit *= 2
        return flipped

    def target_at(step):
        if pairs > 0:
            return lax.rem(my_pair + pairs - step, pairs)
        return pair_at(step)

    for step in range(1, pairs):
        target_pair = target_at(step)
        for core in range(2):
            expert = target_pair * 2 + core
            outgoing[expert] = jnp.dot(
                select_ref[expert], narrow, preferred_element_type=f32
            ).astype(bf16)
    sibling = my_pair * 2 + 1 - my_core
    wide = normed[...]
    for_sibling = jnp.dot(select_ref[sibling], wide, preferred_element_type=f32).astype(bf16)
    for_self = jnp.dot(select_ref[me], wide, preferred_element_type=f32).astype(bf16)
    my_rows = pl.ds(pl.multiple_of(my_core * slots, slots), slots)
    for y in range(ny):
        for x in range(nx):
            begin = (y * nx + x) * columns
            sibling_out[y, x] = for_sibling[:, begin : begin + columns]
            rows_in[my_pair, y, x, my_rows, :] = for_self[:, begin : begin + columns]
    pl.semaphore_wait(barrier, len(greeted))

    start(
        sibling_out,
        rows_in.at[my_pair, :, :, my_rows],
        go_send.at[sibling],
        go_recv.at[me],
        device_at(sibling, my_y, my_x),
    )
    for step in range(1, pairs):
        target_pair = target_at(step)
        for core in range(2):
            expert = target_pair * 2 + core
            start(
                outgoing.at[expert],
                rows_in.at[my_pair, my_y, my_x, my_rows],
                go_send.at[expert],
                go_recv.at[me],
                device_at(expert, my_y, my_x),
            )

    group_width = pool_weight_ref.shape[0]
    group = shard * pool_weight_ref.shape[1] // group_width
    pool_rows = pool_in_ref.shape[0]
    halo_count = pool_tail.shape[0]

    def pool_start():
        inputs = pool_in_ref[...].astype(f32)
        spread = lax.rsqrt(jnp.mean(inputs * inputs, axis=-1, keepdims=True) + EPSILON)
        group_columns = pl.ds(pl.multiple_of(group * group_width, group_width), group_width)
        own = pool_in_ref[:, group_columns].astype(f32)
        pool_own[...] = (own * spread * pool_gain_ref[:, group_columns]).astype(bf16)
        pool_tail[...] = pool_own[pool_rows - halo_count :, :]
        start(
            pool_tail,
            pool_halo,
            halo_sem.at[0],
            halo_sem.at[1],
            device_at(lax.rem(me + 1, experts), my_y, my_x),
        )

    def pool_end():
        arrive(pool_halo, halo_sem.at[0], halo_sem.at[1])
        own = pool_own[...].astype(f32)
        halo = jnp.where(me == 0, 0.0, pool_halo[...].astype(f32))
        current = jnp.concatenate([halo, own], axis=0)
        chosen = jnp.zeros_like(current)
        for number in range(4):
            current = current + pltpu.roll(current, 1 << number, 0)
            chosen = jnp.where(group == number, current, chosen)
        window = jnp.where(group == 0, 2, jnp.where(group == 1, 4, jnp.where(group == 2, 8, 16)))
        position = me * pool_rows + lax.broadcasted_iota(jnp.int32, (pool_rows, 1), 0)
        counts = jnp.minimum(position + 1, window).astype(f32)
        mixed = (chosen[halo_count:] / counts - own).astype(bf16)
        product = jnp.dot(mixed, pool_weight_ref[...], preferred_element_type=f32)
        pool_out_ref[...] = (product * pool_scale_ref[...]).astype(bf16)

    sibling_rows = pl.ds(pl.multiple_of((1 - my_core) * slots, slots), slots)

    def rows_of(core):
        return pl.ds(core * slots, slots)

    def spread_first(step):
        pair = pair_at(step)
        for core in range(2):
            block = rows_in.at[pair, my_y, my_x, rows_of(core)]
            source = pair * 2 + core
            arrive(block, go_send.at[source], go_recv.at[source])
            if core == 0:
                for x in others_x:
                    start(block, block, a0_send.at[pair, x], a0_recv.at[pair, my_x], device_at(me, my_y, x))
            else:
                for y in others_y:
                    start(block, block, a1_send.at[pair, y], a1_recv.at[pair, my_y], device_at(me, y, my_x))

    def spread_second(step):
        pair = pair_at(step)
        for x in others_x:
            arrive(rows_in.at[pair, my_y, x, rows_of(0)], a0_send.at[pair, x], a0_recv.at[pair, x])
        held = rows_in.at[pair, my_y, :, rows_of(0)]
        for y in others_y:
            start(held, held, b0_send.at[pair, y], b0_recv.at[pair, my_y], device_at(me, y, my_x))
        for y in others_y:
            arrive(rows_in.at[pair, y, my_x, rows_of(1)], a1_send.at[pair, y], a1_recv.at[pair, y])
        held = rows_in.at[pair, :, my_x, rows_of(1)]
        for x in others_x:
            start(held, held, b1_send.at[pair, x], b1_recv.at[pair, my_x], device_at(me, my_y, x))

    def spread_end(step):
        pair = pair_at(step)
        for y in others_y:
            arrive(rows_in.at[pair, y, :, rows_of(0)], b0_send.at[pair, y], b0_recv.at[pair, y])
        for x in others_x:
            arrive(rows_in.at[pair, :, x, rows_of(1)], b1_send.at[pair, x], b1_recv.at[pair, x])

    def multiply(step):
        pair = pair_at(step)
        if step == 0:
            arrive(
                rows_in.at[my_pair, :, :, sibling_rows],
                go_send.at[sibling],
                go_recv.at[sibling],
            )
            for copy in weight_copies:
                copy.wait()
        entire = jnp.concatenate(
            [rows_in[pair, y, x] for y in range(ny) for x in range(nx)], axis=1
        )
        gate_part = jnp.dot(entire, gate_ref[...], preferred_element_type=f32)
        up_part = jnp.dot(entire, up_ref[...], preferred_element_type=f32)
        hidden = (gate_part / (1.0 + jnp.exp(-gate_part)) * up_part).astype(bf16)
        for y in range(ny):
            for x in range(nx):
                begin = (y * nx + x) * columns
                parts[pair, y, x] = lax.dot_general(
                    hidden,
                    down_ref[begin : begin + columns, :],
                    (((1,), (1,)), ((), ())),
                    preferred_element_type=f32,
                ).astype(bf16)

    def send_parts(step):
        pair = pair_at(step)
        for x in others_x:
            start(
                parts.at[pair, :, x, rows_of(0)],
                first_in0.at[pair, my_x],
                ra0_send.at[pair, x],
                ra0_recv.at[pair, my_x],
                device_at(me, my_y, x),
            )
        for y in others_y:
            start(
                parts.at[pair, y, :, rows_of(1)],
                first_in1.at[pair, my_y],
                ra1_send.at[pair, y],
                ra1_recv.at[pair, my_y],
                device_at(me, y, my_x),
            )

    def reduce_first(step):
        pair = pair_at(step)
        for x in others_x:
            arrive(first_in0.at[pair, x], ra0_send.at[pair, x], ra0_recv.at[pair, x])
        for y in range(ny):
            total = parts[pair, y, my_x, rows_of(0), :].astype(f32)
            for x in others_x:
                total += first_in0[pair, x, y].astype(f32)
            half_sum0[pair, y] = total.astype(bf16)
        for y in others_y:
            start(
                half_sum0.at[pair, y],
                second_in0.at[pair, my_y],
                rb0_send.at[pair, y],
                rb0_recv.at[pair, my_y],
                device_at(me, y, my_x),
            )
        for y in others_y:
            arrive(first_in1.at[pair, y], ra1_send.at[pair, y], ra1_recv.at[pair, y])
        for x in range(nx):
            total = parts[pair, my_y, x, rows_of(1), :].astype(f32)
            for y in others_y:
                total += first_in1[pair, y, x].astype(f32)
            half_sum1[pair, x] = total.astype(bf16)
        for x in others_x:
            start(
                half_sum1.at[pair, x],
                second_in1.at[pair, my_x],
                rb1_send.at[pair, x],
                rb1_recv.at[pair, my_x],
                device_at(me, my_y, x),
            )

    def reduce_second(step):
        pair = pair_at(step)
        for y in others_y:
            arrive(second_in0.at[pair, y], rb0_send.at[pair, y], rb0_recv.at[pair, y])
        total = half_sum0[pair, my_y].astype(f32)
        for y in others_y:
            total += second_in0[pair, y].astype(f32)
        finished[pair * 2] = total.astype(bf16)
        for x in others_x:
            arrive(second_in1.at[pair, x], rb1_send.at[pair, x], rb1_recv.at[pair, x])
        total = half_sum1[pair, my_x].astype(f32)
        for x in others_x:
            total += second_in1[pair, x].astype(f32)
        finished[pair * 2 + 1] = total.astype(bf16)
        if step == 0:
            targets = [sibling]
            returned[me] = finished[me]
        else:
            targets = [pair * 2, pair * 2 + 1]
        for target in targets:
            start(
                finished.at[target],
                returned.at[me],
                back_send.at[target],
                back_recv.at[me],
                device_at(target, my_y, my_x),
            )

    schedule = [(multiply, (0,)), (send_parts, (0,)), (pool_start, ())]
    for turn in range(1, pairs + 4):
        if turn < pairs:
            schedule += [(spread_first, (turn,))]
        if 1 <= turn - 1 < pairs:
            schedule += [(spread_second, (turn - 1,))]
        if turn == 2:
            schedule += [(pool_end, ())]
        if 1 <= turn - 2 < pairs:
            schedule += [(spread_end, (turn - 2,)), (multiply, (turn - 2,)), (send_parts, (turn - 2,))]
        if 0 <= turn - 3 < pairs:
            schedule += [(reduce_first, (turn - 3,))]
        if 0 <= turn - 4 < pairs:
            schedule += [(reduce_second, (turn - 4,))]
    for action, arguments in schedule:
        action(*arguments)
    total = jnp.dot(blend_ref[me], returned[me], preferred_element_type=f32)
    for step in range(1, experts):
        source = lax.rem(me + step, experts)
        arrive(returned.at[source], back_send.at[source], back_recv.at[source])
        total += jnp.dot(blend_ref[source], returned[source], preferred_element_type=f32)
    out_ref[...] = total.astype(bf16)
    for copy in pending:
        copy.wait_send()


def local(
    pool_input,
    pool_gain,
    pool_weight,
    pool_scale,
    moe_input,
    moe_gain,
    routes,
    route_logits,
    gate_weight,
    up_weight,
    down_weight,
):
    local_rows, row_width = moe_input.shape
    picks_count = routes.shape[1]
    experts, shards = lax.axis_size("ep"), lax.axis_size("tp")
    capacity = 2 * local_rows * picks_count // experts
    slots = -(-capacity // 16) * 16
    columns = row_width // shards
    ny = max(d for d in range(1, shards + 1) if shards % d == 0 and d * d <= shards)
    nx = shards // ny
    pairs = experts // 2
    hidden_units = gate_weight.shape[2]

    expert_ids = jnp.arange(experts, dtype=jnp.int32)
    named = (routes[:, :, None] == expert_ids).astype(jnp.float32)
    visits = jnp.sum(named, axis=1)
    order = jnp.arange(local_rows, dtype=jnp.int32)
    earlier = (order[:, None] > order[None, :]).astype(jnp.float32)
    rank = jnp.dot(earlier, visits, preferred_element_type=jnp.float32).astype(jnp.int32)
    raised = jnp.exp(route_logits)
    shares = raised / jnp.sum(raised, axis=-1, keepdims=True)
    share_of = jnp.sum(named * shares[:, :, None], axis=1)
    slot_ids = jnp.arange(slots, dtype=jnp.int32)
    rank_of, visits_of = rank.T, visits.T
    select = jnp.where(
        rank_of[:, None, :] == slot_ids[None, :, None], visits_of[:, None, :], 0.0
    ).astype(jnp.bfloat16)
    blend = jnp.where(
        rank_of[:, :, None] == slot_ids[None, None, :], share_of.T[:, :, None], 0.0
    ).astype(jnp.bfloat16)

    bf16 = jnp.bfloat16
    dma = pltpu.SemaphoreType.DMA
    vmem = pl.BlockSpec(memory_space=pltpu.VMEM)
    anywhere = pl.BlockSpec(memory_space=pl.ANY)
    block = (slots, columns)
    sems_x, sems_y = dma((pairs, nx)), dma((pairs, ny))
    expert_out, pool_out = pl.pallas_call(
        functools.partial(expert_kernel, (experts, ny, nx, slots, columns)),
        out_shape=(
            jax.ShapeDtypeStruct((local_rows, columns), bf16),
            jax.ShapeDtypeStruct((pool_input.shape[0], pool_weight.shape[1]), bf16),
        ),
        in_specs=[vmem] * 4 + [anywhere] * 3 + [vmem] * 4,
        out_specs=(vmem, vmem),
        scratch_shapes=[
            pltpu.VMEM((local_rows, row_width), bf16),
            pltpu.VMEM((experts,) + block, bf16),
            pltpu.VMEM((ny, nx) + block, bf16),
            pltpu.VMEM((pairs, ny, nx, 2 * slots, columns), bf16),
            pltpu.VMEM((pairs, ny, nx, 2 * slots, columns), bf16),
            pltpu.VMEM((pairs, nx, ny) + block, bf16),
            pltpu.VMEM((pairs, ny, nx) + block, bf16),
            pltpu.VMEM((pairs, ny) + block, bf16),
            pltpu.VMEM((pairs, nx) + block, bf16),
            pltpu.VMEM((pairs, ny) + block, bf16),
            pltpu.VMEM((pairs, nx) + block, bf16),
            pltpu.VMEM((experts,) + block, bf16),
            pltpu.VMEM((experts,) + block, bf16),
            pltpu.VMEM((row_width, hidden_units), bf16),
            pltpu.VMEM((row_width, hidden_units), bf16),
            pltpu.VMEM((row_width, hidden_units), bf16),
            pltpu.VMEM((pool_input.shape[0], pool_weight.shape[0]), bf16),
            pltpu.VMEM((halo_rows, pool_weight.shape[0]), bf16),
            pltpu.VMEM((halo_rows, pool_weight.shape[0]), bf16),
            dma((3,)),
            dma((2,)),
            dma((experts,)),
            dma((experts,)),
        ]
        + [sems_x, sems_x, sems_y, sems_y, sems_y, sems_y, sems_x, sems_x] * 2
        + [dma((experts,)), dma((experts,))],
        compiler_params=pltpu.CompilerParams(
            collective_id=0, has_side_effects=True, vmem_limit_bytes=58 * 1024 * 1024
        ),
    )(
        moe_input,
        moe_gain.reshape(1, row_width),
        select,
        blend,
        gate_weight,
        up_weight,
        down_weight,
        pool_input,
        pool_gain.reshape(1, row_width),
        pool_weight,
        pool_scale.reshape(1, -1),
    )
    return (pool_out, expert_out)


def solution(mesh):
    in_specs = (
        P("ep", None),
        P(),
        P(None, "tp"),
        P("tp"),
        P("ep", None),
        P(),
        P("ep", None),
        P("ep", None),
        P("ep", None, "tp"),
        P("ep", None, "tp"),
        P("ep", None, "tp"),
    )
    out_specs = (P("ep", "tp"), P("ep", "tp"))
    return jax.shard_map(local, mesh=mesh, in_specs=in_specs, out_specs=out_specs, check_vma=False)
```

profile of v0, /device:TPU:1, one launch (start us, length us, event | category | flops | bytes accessed | tf_op | source)
XLA Modules:
  0.0 82.0 jit_solution(10376114398615113128)
XLA Ops:
  0.6 0.7 exponential_reduce_fusion
  1.3 0.7 exponential_divide_fusion
  2.0 0.7 select_reduce_fusion
  2.7 0.1 convolution_convert_fusion
  2.9 1.3 %select_convert_fusion.blend_ref = bf16[8,192,96]{2,1,0:T(8,128)(2,1)} fusion(bf16[8,192]{1,0:T(8,128)(2,1)S(1)} %bitcast.7, s32[8,192]{1,0:T(8,128)S(1)} %convolution_convert_fusion), kind=kLoop, calls=%fused_computation.1 | loop fusion | flops 294912 | bytes 304128 | tf_op jit(solution)/shard_map/convert_element_type | solution.py:425
  4.1 0.9 %select_convert_fusion.1.select_ref = bf16[8,96,192]{2,1,0:T(8,128)(2,1)} fusion(bf16[8,192]{1,0:T(8,128)(2,1)S(1)} %bitcast.6, s32[8,192]{1,0:T(8,128)S(1)} %convolution_convert_fusion), kind=kLoop, calls=%fused_computation.3 | loop fusion | flops 294912 | bytes 304128 | tf_op jit(solution)/shard_map/convert_element_type | solution.py:422
  5.0 73.7 %shard_map.122 = (bf16[192,512]{1,0:T(8,128)(2,1)}, bf16[256,512]{1,0:T(8,128)(2,1)}) custom-call(bf16[192,2048]{1,0:T(8,128)(2,1)} %tokens_ref.1, f32[1,2048]{1,0:T(1,128)} %bitcast.8, bf16[8,96,192]{2,1,0:T(8,128)(2,1)} %select_convert_fusion.1.select_ref, bf16[8,192,96]{2,1,0:T(8,128)(2,1)} %select_convert_fusion.blend_ref, ...), custom_call_target="tpu_custom_call" | custom-call | tf_op jit(solution)/shard_map/pallas_call | solution.py:433
  78.7 1.7 %copy.17 = bf16[256,512]{1,0:T(8,128)(2,1)} copy(bf16[256,512]{1,0:T(8,128)(2,1)} %get-tuple-element.10) | data formatting | bytes 524288
  80.4 1.6 %copy.18 = bf16[192,512]{1,0:T(8,128)(2,1)} copy(bf16[192,512]{1,0:T(8,128)(2,1)} %get-tuple-element.11) | data formatting | bytes 393216
where the time goes:
time: 82.4 us; the launch traced here: 82 us
  Pallas kernels  73.7 us (89%)
  other arithmetic  4.22 us (5%)
  local copies, waits for them, and re-layouts  3.29 us (4%)
    pallas_call x1, Pallas kernels, local(): pl.pallas_call(functools.partial(expert_kernel, (experts, ny, nx, slots,...  73.7 us
    unnamed x2, local copies, waits for them, and re-layouts  3.29 us

commit v1 on v0

v1 whole, which is shorter than its diff:
```python
import functools

import jax
import jax.numpy as jnp
from jax import lax
from jax.experimental import pallas as pl
from jax.experimental.pallas import tpu as pltpu
from jax.sharding import PartitionSpec as P

EPSILON = 1e-06
halo_rows = 16


def plane_orders(planes):
    if planes == 4:
        return [[1, 3, 2], [0, 2, 3], [3, 1, 0], [2, 0, 1]]
    return [[(p + step) % planes for step in range(1, planes)] for p in range(planes)]


FOUR_PLANES = (
    "ZS10", "ZS20", "PS00", "ZS30", "SF11", "OWN00", "SF10", "ZD10", "GU01", "SF21", "GU00",
    "SF20", "DN00", "SP00", "SS21", "SS20", "SF31", "ZD30", "SF30", "SE20", "GU20", "GU21",
    "SE10", "DN20", "SP20", "GU11", "DN21", "SP21", "GU10", "DN01", "DN10", "RF21", "SE30",
    "RF20", "SP10", "PE00", "GU30", "GU31", "DN30", "SP30", "R221", "R220", "DN31", "SP31",
    "RF31", "RF30", "DN11", "RF10", "SP11", "RF11", "RF00", "R231", "SP01", "RF01", "R230",
    "R210", "R211", "R200", "R201",
)
FAR_STEPS = (1, 3,)


def plan(pairs):
    if pairs == 4:
        return [(word[:-2], int(word[-2]), int(word[-1])) for word in FOUR_PLANES]
    order = [("ZS", step, 0) for step in range(1, pairs)]
    order += [("ZD", step, 0) for step in range(1, pairs)]
    order += [("PS", 0, 0), ("OWN", 0, 0), ("GU", 0, 0), ("GU", 0, 1), ("DN", 0, 0), ("DN", 0, 1)]
    for step in range(1, pairs):
        order += [("SF", step, 0), ("SF", step, 1), ("SS", step, 0), ("SS", step, 1), ("SE", step, 0)]
        order += [("GU", step, 0), ("GU", step, 1), ("DN", step, 0), ("DN", step, 1)]
        order += [("SP", step, 0), ("SP", step, 1), ("RF", step, 0), ("RF", step, 1)]
        order += [("R2", step, 0), ("R2", step, 1)]
    order += [("PE", 0, 0), ("SP", 0, 0), ("SP", 0, 1), ("RF", 0, 0), ("RF", 0, 1)]
    return order + [("R2", 0, 0), ("R2", 0, 1)]


def expert_kernel(
    sizes,
    routes_hbm,
    logits_hbm,
    gain_hbm,
    pool_gain_hbm,
    pool_scale_hbm,
    tokens_hbm,
    gate_hbm,
    up_hbm,
    down_hbm,
    pool_in_hbm,
    pool_weight_hbm,
    out_ref,
    pool_out_ref,
    routes_ref,
    logits_ref,
    gain_ref,
    pool_gain_ref,
    pool_scale_ref,
    tokens_ref,
    pool_in_ref,
    pool_weight_ref,
    rank_ref,
    blend_ref,
    normed,
    outgoing,
    outgoing_far,
    sibling_out,
    rows_in,
    hidden_ref,
    parts,
    first_in0,
    first_in1,
    half_sum0,
    half_sum1,
    second_in0,
    second_in1,
    finished,
    returned,
    gate_ref,
    up_ref,
    down_ref,
    pool_own,
    pool_tail,
    pool_halo,
    load_sem,
    halo_sem,
    go_send,
    go_recv,
    far_send,
    spread_send,
    spread_recv,
    ra0_send,
    ra0_recv,
    ra1_send,
    ra1_recv,
    rb0_send,
    rb0_recv,
    rb1_send,
    rb1_recv,
    back_send,
    back_recv,
):
    experts, ny, nx, slots, columns = sizes
    pairs = experts // 2
    me, shard = lax.axis_index("ep"), lax.axis_index("tp")
    my_pair, my_core = me // 2, me % 2
    my_y, my_x = shard // nx, shard % nx
    bf16, f32 = jnp.bfloat16, jnp.float32
    pending = []

    def device_at(ep, y, x):
        return {"ep": ep, "tp": y * nx + x}

    def copy_to(src, dst, send, recv, target):
        return pltpu.make_async_remote_copy(
            src_ref=src,
            dst_ref=dst,
            send_sem=send,
            recv_sem=recv,
            device_id=target,
            device_id_type=pl.DeviceIdType.MESH,
        )

    def start(*arguments):
        copy = copy_to(*arguments)
        copy.start()
        pending.append(copy)

    def arrive(ref, send, recv):
        copy_to(ref, ref, send, recv, device_at(me, my_y, my_x)).wait_recv()

    others_x = [lax.rem(my_x + step, nx) for step in range(1, nx)]
    others_y = [lax.rem(my_y + step, ny) for step in range(1, ny)]
    barrier = pltpu.get_barrier_semaphore()
    greeted = [device_at(lax.rem(me + step, experts), my_y, my_x) for step in range(1, experts)]
    greeted += [device_at(me, my_y, x) for x in others_x]
    greeted += [device_at(me, y, my_x) for y in others_y]
    for target in greeted:
        pl.semaphore_signal(
            barrier, inc=1, device_id=target, device_id_type=pl.DeviceIdType.MESH
        )
    loads = [
        pltpu.make_async_copy(source, target, load_sem.at[number])
        for number, (source, target) in enumerate(
            (
                (routes_hbm, routes_ref),
                (gain_hbm, gain_ref),
                (logits_hbm, logits_ref),
                (pool_gain_hbm, pool_gain_ref),
                (pool_scale_hbm, pool_scale_ref),
                (tokens_hbm, tokens_ref),
                (gate_hbm.at[0], gate_ref),
                (up_hbm.at[0], up_ref),
                (down_hbm.at[0], down_ref),
                (pool_in_hbm, pool_in_ref),
                (pool_weight_hbm, pool_weight_ref),
            )
        )
    ]
    load_small = loads[:5]
    load_tokens, load_gate, load_up, load_down, load_pool_in, load_pool_weight = loads[5:]
    for copy in load_small:
        copy.start()
    load_tokens.start()
    load_pool_in.start()
    load_gate.start()
    load_up.start()
    load_down.start()
    load_pool_weight.start()

    is_plane = [
        1 - ((my_pair - p) * (my_pair - p) + pairs * pairs - 1) // (pairs * pairs)
        for p in range(pairs)
    ]
    orders = plane_orders(pairs)
    pair_of = [my_pair]
    for step in range(1, pairs):
        number = 0
        for p in range(pairs):
            if orders[p][step - 1]:
                number = number + is_plane[p] * orders[p][step - 1]
        pair_of.append(number)

    for copy in load_small:
        copy.wait()
    tokens_count, picks = routes_ref.shape[1], routes_ref.shape[0]
    expert_ids = lax.broadcasted_iota(jnp.int32, (experts, tokens_count), 0)
    named = [
        jnp.where(routes_ref[pick : pick + 1, :] == expert_ids, 1.0, 0.0) for pick in range(picks)
    ]
    visits = functools.reduce(jnp.add, named)
    earlier = (
        lax.broadcasted_iota(jnp.int32, (tokens_count, tokens_count), 0)
        < lax.broadcasted_iota(jnp.int32, (tokens_count, tokens_count), 1)
    )
    rank = jnp.dot(
        visits.astype(bf16), jnp.where(earlier, 1.0, 0.0).astype(bf16), preferred_element_type=f32
    )
    rank_ref[...] = jnp.where(visits > 0.5, rank, -1.0)
    slot_ids = lax.broadcasted_iota(jnp.int32, (slots, tokens_count), 0).astype(f32)

    def select(expert):
        return jnp.where(rank_ref[pl.ds(expert, 1), :] == slot_ids, 1.0, 0.0)

    def select_two(first, second):
        return jnp.concatenate([select(first), select(second)], axis=0).astype(bf16)

    load_tokens.wait()
    values = tokens_ref[...].astype(f32)
    scale = lax.rsqrt(jnp.mean(values * values, axis=-1, keepdims=True) + EPSILON)
    normed[...] = (values * scale * gain_ref[...]).astype(bf16)
    own_columns = pl.ds(pl.multiple_of(shard * columns, columns), columns)
    far_of = [(y, x) for y in others_y for x in others_x]

    def columns_of(y, x):
        return pl.ds(pl.multiple_of((y * nx + x) * columns, columns), columns)

    for step in range(1, pairs):
        pair = pair_of[step]
        chosen_rows = select_two(pair * 2, pair * 2 + 1)
        targets = [(own_columns, outgoing)]
        if step in FAR_STEPS:
            targets += [
                (columns_of(y, x), outgoing_far.at[number]) for number, (y, x) in enumerate(far_of)
            ]
        for where, target in targets:
            picked = jnp.dot(
                chosen_rows, normed[:, where], preferred_element_type=f32
            ).astype(bf16)
            target[pair * 2] = picked[:slots]
            target[pair * 2 + 1] = picked[slots:]
    sibling = my_pair * 2 + 1 - my_core
    for_both = jnp.dot(
        select_two(sibling, me), normed[...], preferred_element_type=f32
    ).astype(bf16)
    my_rows = pl.ds(pl.multiple_of(my_core * slots, slots), slots)
    for y in range(ny):
        for x in range(nx):
            begin = (y * nx + x) * columns
            sibling_out[y, x] = for_both[:slots, begin : begin + columns]
            rows_in[my_pair, y, x, my_rows, :] = for_both[slots:, begin : begin + columns]
    pl.semaphore_wait(barrier, len(greeted))

    start(
        sibling_out,
        rows_in.at[my_pair, :, :, my_rows],
        go_send.at[sibling],
        go_recv.at[me],
        device_at(sibling, my_y, my_x),
    )

    group_width = pool_weight_ref.shape[0]
    group = shard * pool_weight_ref.shape[1] // group_width
    pool_rows = pool_in_ref.shape[0]
    halo_count = pool_tail.shape[0]

    def pool_start(*_):
        load_pool_in.wait()
        inputs = pool_in_ref[...].astype(f32)
        spread = lax.rsqrt(jnp.mean(inputs * inputs, axis=-1, keepdims=True) + EPSILON)
        group_columns = pl.ds(pl.multiple_of(group * group_width, group_width), group_width)
        own = pool_in_ref[:, group_columns].astype(f32)
        pool_own[...] = (own * spread * pool_gain_ref[:, group_columns]).astype(bf16)
        pool_tail[...] = pool_own[pool_rows - halo_count :, :]
        start(
            pool_tail,
            pool_halo,
            halo_sem.at[0],
            halo_sem.at[1],
            device_at(lax.rem(me + 1, experts), my_y, my_x),
        )
        raised = jnp.exp(logits_ref[...])
        shares = raised / jnp.sum(raised, axis=0, keepdims=True)
        share_of = functools.reduce(
            jnp.add, [named[pick] * shares[pick : pick + 1, :] for pick in range(picks)]
        )
        weighted = [
            jnp.where(rank_ref[e : e + 1, :] == slot_ids, share_of[e : e + 1, :], 0.0)
            for e in range(experts)
        ]
        blend_ref[...] = jnp.concatenate(weighted, axis=0).T.astype(bf16)

    def pool_end(*_):
        load_pool_weight.wait()
        arrive(pool_halo, halo_sem.at[0], halo_sem.at[1])
        own = pool_own[...].astype(f32)
        halo = jnp.where(me == 0, 0.0, pool_halo[...].astype(f32))
        current = jnp.concatenate([halo, own], axis=0)
        chosen = jnp.zeros_like(current)
        for number in range(4):
            current = current + pltpu.roll(current, 1 << number, 0)
            chosen = jnp.where(group == number, current, chosen)
        window = jnp.where(group == 0, 2, jnp.where(group == 1, 4, jnp.where(group == 2, 8, 16)))
        position = me * pool_rows + lax.broadcasted_iota(jnp.int32, (pool_rows, 1), 0)
        counts = jnp.minimum(position + 1, window).astype(f32)
        mixed = (chosen[halo_count:] / counts - own).astype(bf16)
        product = jnp.dot(mixed, pool_weight_ref[...], preferred_element_type=f32)
        pool_out_ref[...] = (product * pool_scale_ref[...]).astype(bf16)

    sibling_rows = pl.ds(pl.multiple_of((1 - my_core) * slots, slots), slots)

    def rows_of(core):
        return pl.ds(core * slots, slots)

    def own_rows(*_):
        arrive(
            rows_in.at[my_pair, :, :, sibling_rows], go_send.at[sibling], go_recv.at[sibling]
        )
        load_gate.wait()
        load_up.wait()

    def spread_recv_of(pair, core, y, x):
        return spread_recv.at[(pair * 2 + core) * ny + y, x]

    def spread_send_of(pair, core, y, x):
        return spread_send.at[(pair * 2 + core) * ny + y, x]

    def go_own(step, _):
        for core in range(2):
            expert = pair_of[step] * 2 + core
            start(
                outgoing.at[expert],
                rows_in.at[my_pair, my_y, my_x, my_rows],
                go_send.at[expert],
                go_recv.at[me],
                device_at(expert, my_y, my_x),
            )

    def go_far(step, _):
        if step not in FAR_STEPS:
            return
        for core in range(2):
            expert = pair_of[step] * 2 + core
            for number, (y, x) in enumerate(far_of):
                start(
                    outgoing_far.at[number, expert],
                    rows_in.at[my_pair, y, x, my_rows],
                    far_send.at[number, expert],
                    spread_recv.at[me * ny + y, x],
                    device_at(expert, my_y, my_x),
                )

    def spread_own(step, core):
        pair = pair_of[step]
        block = rows_in.at[pair, my_y, my_x, rows_of(core)]
        source = pair * 2 + core
        arrive(block, go_send.at[source], go_recv.at[source])
        mine = spread_recv_of(pair, core, my_y, my_x)
        for x in others_x:
            start(block, block, spread_send_of(pair, core, my_y, x), mine, device_at(me, my_y, x))
        for y in others_y:
            start(block, block, spread_send_of(pair, core, y, my_x), mine, device_at(me, y, my_x))

    def take(step, core, y, x):
        pair = pair_of[step]
        arrive(
            rows_in.at[pair, y, x, rows_of(core)],
            spread_send_of(pair, core, y, x),
            spread_recv_of(pair, core, y, x),
        )

    def relay(step, core):
        pair = pair_of[step]
        if step in FAR_STEPS:
            return
        if core == 0:
            for x in others_x:
                take(step, core, my_y, x)
                block = rows_in.at[pair, my_y, x, rows_of(core)]
                arrived = spread_recv_of(pair, core, my_y, x)
                for y in others_y:
                    start(block, block, spread_send_of(pair, core, y, x), arrived, device_at(me, y, my_x))
        else:
            for y in others_y:
                take(step, core, y, my_x)
                block = rows_in.at[pair, y, my_x, rows_of(core)]
                arrived = spread_recv_of(pair, core, y, my_x)
                for x in others_x:
                    start(block, block, spread_send_of(pair, core, y, x), arrived, device_at(me, my_y, x))

    def spread_end(step, _):
        for core in range(2):
            relayed = step not in FAR_STEPS
            if not (relayed and core == 0):
                for x in others_x:
                    take(step, core, my_y, x)
            if not (relayed and core == 1):
                for y in others_y:
                    take(step, core, y, my_x)
            for y, x in far_of:
                take(step, core, y, x)

    hidden_half = gate_ref.shape[1] // 2

    def gate_up(step, half):
        pair = pair_of[step]
        entire = jnp.concatenate(
            [rows_in[pair, y, x] for y in range(ny) for x in range(nx)], axis=1
        )
        where = pl.ds(half * hidden_half, hidden_half)
        gate_part = jnp.dot(entire, gate_ref[:, where], preferred_element_type=f32)
        up_part = jnp.dot(entire, up_ref[:, where], preferred_element_type=f32)
        hidden_ref[step, :, where] = (
            gate_part / (1.0 + jnp.exp(-gate_part)) * up_part
        ).astype(bf16)

    def down(step, part):
        pair = pair_of[step]
        if step == 0 and part == 0:
            load_down.wait()
        hidden = hidden_ref[step]
        blocks = far_of
        if part:
            blocks = [(my_y, x) for x in others_x] + [(y, my_x) for y in others_y] + [(my_y, my_x)]
        for y, x in blocks:
            parts[pair, y, x] = lax.dot_general(
                hidden,
                down_ref[columns_of(y, x), :],
                (((1,), (1,)), ((), ())),
                preferred_element_type=f32,
            ).astype(bf16)

    def send_parts(step, part):
        pair = pair_of[step]
        for y in [my_y] if part else others_y:
            for x in others_x:
                start(
                    parts.at[pair, y, x, rows_of(0)],
                    first_in0.at[pair, my_x, y],
                    ra0_send.at[pair * nx + x, y],
                    ra0_recv.at[pair * nx + my_x, y],
                    device_at(me, my_y, x),
                )
        for x in [my_x] if part else others_x:
            for y in others_y:
                start(
                    parts.at[pair, y, x, rows_of(1)],
                    first_in1.at[pair, my_y, x],
                    ra1_send.at[pair * ny + y, x],
                    ra1_recv.at[pair * ny + my_y, x],
                    device_at(me, y, my_x),
                )

    def summed0(pair, y):
        total = parts[pair, y, my_x, rows_of(0), :].astype(f32)
        for x in others_x:
            arrive(
                first_in0.at[pair, x, y], ra0_send.at[pair * nx + x, y], ra0_recv.at[pair * nx + x, y]
            )
            total += first_in0[pair, x, y].astype(f32)
        return total

    def summed1(pair, x):
        total = parts[pair, my_y, x, rows_of(1), :].astype(f32)
        for y in others_y:
            arrive(
                first_in1.at[pair, y, x], ra1_send.at[pair * ny + y, x], ra1_recv.at[pair * ny + y, x]
            )
            total += first_in1[pair, y, x].astype(f32)
        return total

    def reduce_first(step, core):
        pair = pair_of[step]
        if core == 0:
            for y in others_y:
                half_sum0[pair, y] = summed0(pair, y).astype(bf16)
                start(
                    half_sum0.at[pair, y],
                    second_in0.at[pair, my_y],
                    rb0_send.at[pair, y],
                    rb0_recv.at[pair, my_y],
                    device_at(me, y, my_x),
                )
        else:
            for x in others_x:
                half_sum1[pair, x] = summed1(pair, x).astype(bf16)
                start(
                    half_sum1.at[pair, x],
                    second_in1.at[pair, my_x],
                    rb1_send.at[pair, x],
                    rb1_recv.at[pair, my_x],
                    device_at(me, my_y, x),
                )

    def slots_of(expert):
        return pl.ds(pl.multiple_of(expert * slots, slots), slots)

    def give_back(target):
        start(
            finished.at[target],
            returned.at[slots_of(me)],
            back_send.at[target],
            back_recv.at[me],
            device_at(target, my_y, my_x),
        )

    def reduce_second(step, core):
        pair = pair_of[step]
        if core == 0:
            total = summed0(pair, my_y)
            for y in others_y:
                arrive(second_in0.at[pair, y], rb0_send.at[pair, y], rb0_recv.at[pair, y])
                total += second_in0[pair, y].astype(f32)
        else:
            total = summed1(pair, my_x)
            for x in others_x:
                arrive(second_in1.at[pair, x], rb1_send.at[pair, x], rb1_recv.at[pair, x])
                total += second_in1[pair, x].astype(f32)
        finished[pair * 2 + core] = total.astype(bf16)
        if step:
            give_back(pair * 2 + core)
        elif core:
            give_back(sibling)
            returned[slots_of(me), :] = finished[me]

    actions = {
        "ZS": go_own,
        "ZD": go_far,
        "PS": pool_start,
        "PE": pool_end,
        "OWN": own_rows,
        "SF": spread_own,
        "SS": relay,
        "SE": spread_end,
        "GU": gate_up,
        "DN": down,
        "SP": send_parts,
        "RF": reduce_first,
        "R2": reduce_second,
    }
    for name, step, part in plan(pairs):
        actions[name](step, part)
    for step in range(1, experts):
        source = lax.rem(me + step, experts)
        arrive(returned.at[slots_of(source)], back_send.at[source], back_recv.at[source])
    out_ref[...] = jnp.dot(blend_ref[...], returned[...], preferred_element_type=f32).astype(bf16)
    for copy in pending:
        copy.wait_send()


def local(
    pool_input,
    pool_gain,
    pool_weight,
    pool_scale,
    moe_input,
    moe_gain,
    routes,
    route_logits,
    gate_weight,
    up_weight,
    down_weight,
):
    local_rows, row_width = moe_input.shape
    picks_count = routes.shape[1]
    experts, shards = lax.axis_size("ep"), lax.axis_size("tp")
    capacity = 2 * local_rows * picks_count // experts
    slots = -(-capacity // 16) * 16
    columns = row_width // shards
    ny = max(d for d in range(1, shards + 1) if shards % d == 0 and d * d <= shards)
    nx = shards // ny
    pairs = experts // 2
    hidden_units = gate_weight.shape[2]
    pool_rows, group_width = pool_input.shape[0], pool_weight.shape[0]

    bf16, f32 = jnp.bfloat16, jnp.float32
    dma = pltpu.SemaphoreType.DMA
    vmem = pl.BlockSpec(memory_space=pltpu.VMEM)
    anywhere = pl.BlockSpec(memory_space=pl.ANY)
    block = (slots, columns)
    sems_x, sems_y = dma((pairs, nx)), dma((pairs, ny))
    spread_sems = dma((experts * ny, nx))
    far_count = (ny - 1) * (nx - 1)
    expert_out, pool_out = pl.pallas_call(
        functools.partial(expert_kernel, (experts, ny, nx, slots, columns)),
        out_shape=(
            pltpu.VMEM((local_rows, columns), bf16),
            pltpu.VMEM((pool_rows, pool_weight.shape[1]), bf16),
        ),
        in_specs=[anywhere] * 11,
        out_specs=(vmem, vmem),
        scratch_shapes=[
            pltpu.VMEM((picks_count, local_rows), jnp.int32),
            pltpu.VMEM((picks_count, local_rows), f32),
            pltpu.VMEM((1, row_width), f32),
            pltpu.VMEM((1, row_width), f32),
            pltpu.VMEM((1, pool_weight.shape[1]), f32),
            pltpu.VMEM((local_rows, row_width), bf16),
            pltpu.VMEM((pool_rows, row_width), bf16),
            pltpu.VMEM(pool_weight.shape, bf16),
            pltpu.VMEM((experts, local_rows), f32),
            pltpu.VMEM((local_rows, experts * slots), bf16),
            pltpu.VMEM((local_rows, row_width), bf16),
            pltpu.VMEM((experts,) + block, bf16),
            pltpu.VMEM((far_count, experts) + block, bf16),
            pltpu.VMEM((ny, nx) + block, bf16),
            pltpu.VMEM((pairs, ny, nx, 2 * slots, columns), bf16),
            pltpu.VMEM((pairs, 2 * slots, hidden_units), bf16),
            pltpu.VMEM((pairs, ny, nx, 2 * slots, columns), bf16),
            pltpu.VMEM((pairs, nx, ny) + block, bf16),
            pltpu.VMEM((pairs, ny, nx) + block, bf16),
            pltpu.VMEM((pairs, ny) + block, bf16),
            pltpu.VMEM((pairs, nx) + block, bf16),
            pltpu.VMEM((pairs, ny) + block, bf16),
            pltpu.VMEM((pairs, nx) + block, bf16),
            pltpu.VMEM((experts,) + block, bf16),
            pltpu.VMEM((experts * slots, columns), bf16),
            pltpu.VMEM((row_width, hidden_units), bf16),
            pltpu.VMEM((row_width, hidden_units), bf16),
            pltpu.VMEM((row_width, hidden_units), bf16),
            pltpu.VMEM((pool_rows, group_width), bf16),
            pltpu.VMEM((halo_rows, group_width), bf16),
            pltpu.VMEM((halo_rows, group_width), bf16),
            dma((11,)),
            dma((2,)),
            dma((experts,)),
            dma((experts,)),
        ]
        + [dma((far_count, experts)), spread_sems, spread_sems]
        + [dma((pairs * nx, ny))] * 2
        + [dma((pairs * ny, nx))] * 2
        + [sems_y, sems_y, sems_x, sems_x]
        + [dma((experts,)), dma((experts,))],
        compiler_params=pltpu.CompilerParams(
            collective_id=0, has_side_effects=True, vmem_limit_bytes=56 * 1024 * 1024
        ),
    )(
        routes.T,
        route_logits.T,
        moe_gain.reshape(1, row_width),
        pool_gain.reshape(1, row_width),
        pool_scale.reshape(1, -1),
        moe_input,
        gate_weight,
        up_weight,
        down_weight,
        pool_input,
        pool_weight,
    )
    return (pool_out, expert_out)


def solution(mesh):
    in_specs = (
        P("ep", None),
        P(),
        P(None, "tp"),
        P("tp"),
        P("ep", None),
        P(),
        P("ep", None),
        P("ep", None),
        P("ep", None, "tp"),
        P("ep", None, "tp"),
        P("ep", None, "tp"),
    )
    out_specs = (P("ep", "tp"), P("ep", "tp"))
    return jax.shard_map(local, mesh=mesh, in_specs=in_specs, out_specs=out_specs, check_vma=False)
```

time: 82.4 us -> 60.1 us (0.73)
  Pallas kernels: 73.7 us -> 57.9 us
  other arithmetic: 4.22 us -> 0 us
  local copies, waits for them, and re-layouts: 3.29 us -> 1.38 us
    pallas_call x1, Pallas kernels: 73.7 us -> 57.9 us  [local(): pl.pallas_call(functools.partial(expert_kernel, (experts, ny, nx, slots,...]
    convert_element_type x2 -> x0, other arithmetic: 2.13 us -> none  [the longest x1 1.28 us: local(): blend = jnp.where(rank_of[:, :, None] == slot_ids[None, None, :], share_o...]
    unnamed x2, local copies, waits for them, and re-layouts: 3.29 us -> 1.38 us
    reduce_sum x2 -> x0, other arithmetic: 1.39 us -> none  [the longest x1 0.7 us: local(): shares = raised / jnp.sum(raised, axis=-1, keepdims=True)]
where the time goes in v1:
time: 60.1 us; the launch traced here: 59.9 us
  Pallas kernels  57.9 us (96%)
  local copies, waits for them, and re-layouts  1.38 us (2%)
  between operations  0.64 us (1%)
    pallas_call x1, Pallas kernels, local(): pl.pallas_call(functools.partial(expert_kernel, (experts, ny, nx, slots,...  57.9 us
    unnamed x2, local copies, waits for them, and re-layouts  1.38 us

profile of v1, /device:TPU:1, one launch (start us, length us, event | category | flops | bytes accessed | tf_op | source)
XLA Modules:
  0.0 59.9 jit_solution(14747608634205142325)
XLA Ops:
  0.6 57.9 %shard_map.122 = (bf16[192,512]{1,0:T(8,128)(2,1)S(1)}, bf16[256,512]{1,0:T(8,128)(2,1)S(1)}) custom-call(s32[2,192]{1,0:T(2,128)} %bitcast.7, f32[2,192]{1,0:T(2,128)} %bitcast.8, f32[1,2048]{1,0:T(1,128)} %bitcast.5, f32[1,2048]{1,0:T(1,128)} %bitcast.6, f32[1,512]{1,0:T(1,128)} %bitcast.9, bf16[192,2048]{1,0:T(8,128)(2,1)} %tokens_hbm.1, ...), custom_call_target="tpu_custom_call" | custom-call | tf_op jit(solution)/shard_map/pallas_call | solution.py:581
  58.5 0.7 %copy.15 = bf16[256,512]{1,0:T(8,128)(2,1)} copy(bf16[256,512]{1,0:T(8,128)(2,1)S(1)} %get-tuple-element.6) | data formatting | bytes 524288
  59.2 0.7 %copy.16 = bf16[192,512]{1,0:T(8,128)(2,1)} copy(bf16[192,512]{1,0:T(8,128)(2,1)S(1)} %get-tuple-element.7) | data formatting | bytes 393216

commit v2 on v1

--- a/solution.py
+++ b/solution.py
@@ -18,21 +18,21 @@
 
 
 FOUR_PLANES = (
-    "ZS10", "ZS20", "PS00", "ZS30", "SF11", "OWN00", "SF10", "ZD10", "GU01", "SF21", "GU00",
-    "SF20", "DN00", "SP00", "SS21", "SS20", "SF31", "ZD30", "SF30", "SE20", "GU20", "GU21",
-    "SE10", "DN20", "SP20", "GU11", "DN21", "SP21", "GU10", "DN01", "DN10", "RF21", "SE30",
-    "RF20", "SP10", "PE00", "GU30", "GU31", "DN30", "SP30", "R221", "R220", "DN31", "SP31",
-    "RF31", "RF30", "DN11", "RF10", "SP11", "RF11", "RF00", "R231", "SP01", "RF01", "R230",
-    "R210", "R211", "R200", "R201",
+    "ZS10", "ZS20", "PS00", "ZS30", "SB00", "SF11", "OWN00", "ZD10", "GU01", "SF10", "SF21",
+    "GU00", "SF20", "DN00", "SP00", "SS21", "SS20", "SF31", "ZD30", "SF30", "SE20", "GU20",
+    "GU21", "SE10", "DN20", "GU11", "SP20", "DN21", "SP21", "GU10", "DN01", "DN10", "RF21",
+    "RF20", "SE30", "SP10", "GU30", "DN11", "GU31", "DN30", "SP30", "R221", "R220", "DN31",
+    "SP31", "RF31", "RF30", "RF10", "SP11", "RF11", "PE00", "RF00", "R231", "SP01", "RF01",
+    "R210", "R230", "R211", "R200", "R201",
 )
-FAR_STEPS = (1, 3,)
+FAR_STEPS = (1, 3)
 
 
 def plan(pairs):
     if pairs == 4:
         return [(word[:-2], int(word[-2]), int(word[-1])) for word in FOUR_PLANES]
     order = [("ZS", step, 0) for step in range(1, pairs)]
-    order += [("ZD", step, 0) for step in range(1, pairs)]
+    order += [("SB", 0, 0)] + [("ZD", step, 0) for step in range(1, pairs)]
     order += [("PS", 0, 0), ("OWN", 0, 0), ("GU", 0, 0), ("GU", 0, 1), ("DN", 0, 0), ("DN", 0, 1)]
     for step in range(1, pairs):
         order += [("SF", step, 0), ("SF", step, 1), ("SS", step, 0), ("SS", step, 1), ("SE", step, 0)]
@@ -81,6 +81,10 @@
     half_sum1,
     second_in0,
     second_in1,
+    own_in0,
+    own_in1,
+    own_part,
+    own_came,
     finished,
     returned,
     gate_ref,
@@ -104,11 +108,17 @@
     rb0_recv,
     rb1_send,
     rb1_recv,
+    own0_send,
+    own0_recv,
+    own1_send,
+    own1_recv,
+    core_sem,
     back_send,
     back_recv,
 ):
     experts, ny, nx, slots, columns = sizes
     pairs = experts // 2
+    far_steps = FAR_STEPS if pairs == 4 else ()
     me, shard = lax.axis_index("ep"), lax.axis_index("tp")
     my_pair, my_core = me // 2, me % 2
     my_y, my_x = shard // nx, shard % nx
@@ -140,8 +150,9 @@
     others_y = [lax.rem(my_y + step, ny) for step in range(1, ny)]
     barrier = pltpu.get_barrier_semaphore()
     greeted = [device_at(lax.rem(me + step, experts), my_y, my_x) for step in range(1, experts)]
-    greeted += [device_at(me, my_y, x) for x in others_x]
-    greeted += [device_at(me, y, my_x) for y in others_y]
+    for ep in (me, my_pair * 2 + 1 - my_core):
+        greeted += [device_at(ep, my_y, x) for x in others_x]
+        greeted += [device_at(ep, y, my_x) for y in others_y]
     for target in greeted:
         pl.semaphore_signal(
             barrier, inc=1, device_id=target, device_id_type=pl.DeviceIdType.MESH
@@ -222,39 +233,36 @@
     def columns_of(y, x):
         return pl.ds(pl.multiple_of((y * nx + x) * columns, columns), columns)
 
-    for step in range(1, pairs):
-        pair = pair_of[step]
-        chosen_rows = select_two(pair * 2, pair * 2 + 1)
-        targets = [(own_columns, outgoing)]
-        if step in FAR_STEPS:
-            targets += [
-                (columns_of(y, x), outgoing_far.at[number]) for number, (y, x) in enumerate(far_of)
-            ]
-        for where, target in targets:
-            picked = jnp.dot(
-                chosen_rows, normed[:, where], preferred_element_type=f32
-            ).astype(bf16)
-            target[pair * 2] = picked[:slots]
-            target[pair * 2 + 1] = picked[slots:]
     sibling = my_pair * 2 + 1 - my_core
-    for_both = jnp.dot(
-        select_two(sibling, me), normed[...], preferred_element_type=f32
-    ).astype(bf16)
     my_rows = pl.ds(pl.multiple_of(my_core * slots, slots), slots)
-    for y in range(ny):
-        for x in range(nx):
-            begin = (y * nx + x) * columns
-            sibling_out[y, x] = for_both[:slots, begin : begin + columns]
-            rows_in[my_pair, y, x, my_rows, :] = for_both[slots:, begin : begin + columns]
     pl.semaphore_wait(barrier, len(greeted))
 
-    start(
-        sibling_out,
-        rows_in.at[my_pair, :, :, my_rows],
-        go_send.at[sibling],
-        go_recv.at[me],
-        device_at(sibling, my_y, my_x),
-    )
+    def pick_rows(step, columns_at, target):
+        pair = pair_of[step]
+        picked = jnp.dot(
+            select_two(pair * 2, pair * 2 + 1),
+            normed[:, columns_at],
+            preferred_element_type=f32,
+        ).astype(bf16)
+        target[pair * 2] = picked[:slots]
+        target[pair * 2 + 1] = picked[slots:]
+
+    def go_sibling(*_):
+        for_both = jnp.dot(
+            select_two(sibling, me), normed[...], preferred_element_type=f32
+        ).astype(bf16)
+        for y in range(ny):
+            for x in range(nx):
+                begin = (y * nx + x) * columns
+                sibling_out[y, x] = for_both[:slots, begin : begin + columns]
+                rows_in[my_pair, y, x, my_rows, :] = for_both[slots:, begin : begin + columns]
+        start(
+            sibling_out,
+            rows_in.at[my_pair, :, :, my_rows],
+            go_send.at[sibling],
+            go_recv.at[me],
+            device_at(sibling, my_y, my_x),
+        )
 
     group_width = pool_weight_ref.shape[0]
     group = shard * pool_weight_ref.shape[1] // group_width
@@ -323,6 +331,7 @@
         return spread_send.at[(pair * 2 + core) * ny + y, x]
 
     def go_own(step, _):
+        pick_rows(step, own_columns, outgoing)
         for core in range(2):
             expert = pair_of[step] * 2 + core
             start(
@@ -334,8 +343,10 @@
             )
 
     def go_far(step, _):
-        if step not in FAR_STEPS:
+        if step not in far_steps:
             return
+        for number, (y, x) in enumerate(far_of):
+            pick_rows(step, columns_of(y, x), outgoing_far.at[number])
         for core in range(2):
             expert = pair_of[step] * 2 + core
             for number, (y, x) in enumerate(far_of):
@@ -368,7 +379,7 @@
 
     def relay(step, core):
         pair = pair_of[step]
-        if step in FAR_STEPS:
+        if step in far_steps:
             return
         if core == 0:
             for x in others_x:
@@ -387,7 +398,7 @@
 
     def spread_end(step, _):
         for core in range(2):
-            relayed = step not in FAR_STEPS
+            relayed = step not in far_steps
             if not (relayed and core == 0):
                 for x in others_x:
                     take(step, core, my_y, x)
@@ -466,9 +477,70 @@
             total += first_in1[pair, y, x].astype(f32)
         return total
 
+    def reduce_own(core):
+        owner = my_pair * 2 + core
+        if core == 0:
+            others = [(half_sum0, summed0, y, device_at(owner, y, my_x)) for y in others_y]
+            arriving, sent, received, here = own_in0, own0_send, own0_recv, my_y
+        else:
+            others = [(half_sum1, summed1, x, device_at(owner, my_y, x)) for x in others_x]
+            arriving, sent, received, here = own_in1, own1_send, own1_recv, my_x
+        for sums, summed, place, target in others:
+            sums[my_pair, place] = summed(my_pair, place).astype(bf16)
+            start(
+                sums.at[my_pair, place],
+                arriving.at[my_core, here],
+                sent.at[place],
+                received.at[my_core, here],
+                target,
+            )
+
+    def keep_own(core):
+        mine = summed1(my_pair, my_x) if core else summed0(my_pair, my_y)
+        own_part[core] = mine.astype(bf16)
+
+        @pl.when(my_core != core)
+        def _():
+            copy_to(
+                own_part.at[core],
+                own_came,
+                core_sem.at[0],
+                core_sem.at[1],
+                device_at(sibling, my_y, my_x),
+            ).start()
+
+    def finish_own():
+        copy_to(
+            own_came, own_came, core_sem.at[0], core_sem.at[1], device_at(me, my_y, my_x)
+        ).wait_recv()
+        for core in range(2):
+
+            @pl.when(my_core == core)
+            def _(core=core):
+                arriving, received, sent, places = (
+                    (own_in0, own0_recv, own0_send, others_y)
+                    if core == 0
+                    else (own_in1, own1_recv, own1_send, others_x)
+                )
+                for source in range(2):
+                    part = own_part[core] if source == core else own_came[...]
+                    total = part.astype(f32)
+                    for place in places:
+                        arrive(
+                            arriving.at[source, place], sent.at[place], received.at[source, place]
+                        )
+                        total += arriving[source, place].astype(f32)
+                    returned[slots_of(my_pair * 2 + source), :] = total.astype(bf16)
+
+        copy_to(
+            own_part.at[0], own_came, core_sem.at[0], core_sem.at[1], device_at(sibling, my_y, my_x)
+        ).wait_send()
+
     def reduce_first(step, core):
         pair = pair_of[step]
-        if core == 0:
+        if step == 0:
+            reduce_own(core)
+        elif core == 0:
             for y in others_y:
                 half_sum0[pair, y] = summed0(pair, y).astype(bf16)
                 start(
@@ -503,6 +575,13 @@
 
     def reduce_second(step, core):
         pair = pair_of[step]
+        if step == 0:
+            if core == 0:
+                keep_own(0)
+                keep_own(1)
+            else:
+                finish_own()
+            return
         if core == 0:
             total = summed0(pair, my_y)
             for y in others_y:
@@ -514,15 +593,12 @@
                 arrive(second_in1.at[pair, x], rb1_send.at[pair, x], rb1_recv.at[pair, x])
                 total += second_in1[pair, x].astype(f32)
         finished[pair * 2 + core] = total.astype(bf16)
-        if step:
-            give_back(pair * 2 + core)
-        elif core:
-            give_back(sibling)
-            returned[slots_of(me), :] = finished[me]
+        give_back(pair * 2 + core)
 
     actions = {
         "ZS": go_own,
         "ZD": go_far,
+        "SB": go_sibling,
         "PS": pool_start,
         "PE": pool_end,
         "OWN": own_rows,
@@ -537,12 +613,26 @@
     }
     for name, step, part in plan(pairs):
         actions[name](step, part)
-    for step in range(1, experts):
-        source = lax.rem(me + step, experts)
-        arrive(returned.at[slots_of(source)], back_send.at[source], back_recv.at[source])
+    for step in range(1, pairs):
+        for core in range(2):
+            source = pair_of[step] * 2 + core
+            arrive(returned.at[slots_of(source)], back_send.at[source], back_recv.at[source])
     out_ref[...] = jnp.dot(blend_ref[...], returned[...], preferred_element_type=f32).astype(bf16)
     for copy in pending:
         copy.wait_send()
+
+
+def store_kernel(pool_ref, expert_ref, pool_hbm, expert_hbm, sems):
+    copies = [
+        pltpu.make_async_copy(source, target, sems.at[number])
+        for number, (source, target) in enumerate(
+            ((pool_ref, pool_hbm), (expert_ref, expert_hbm))
+        )
+    ]
+    for copy in copies:
+        copy.start()
+    for copy in copies:
+        copy.wait()
 
 
 def local(
@@ -610,6 +700,10 @@
             pltpu.VMEM((pairs, nx) + block, bf16),
             pltpu.VMEM((pairs, ny) + block, bf16),
             pltpu.VMEM((pairs, nx) + block, bf16),
+            pltpu.VMEM((2, ny) + block, bf16),
+            pltpu.VMEM((2, nx) + block, bf16),
+            pltpu.VMEM((2,) + block, bf16),
+            pltpu.VMEM(block, bf16),
             pltpu.VMEM((experts,) + block, bf16),
             pltpu.VMEM((experts * slots, columns), bf16),
             pltpu.VMEM((row_width, hidden_units), bf16),
@@ -627,6 +721,7 @@
         + [dma((pairs * nx, ny))] * 2
         + [dma((pairs * ny, nx))] * 2
         + [sems_y, sems_y, sems_x, sems_x]
+        + [dma((ny,)), dma((2, ny)), dma((nx,)), dma((2, nx)), dma((2,))]
         + [dma((experts,)), dma((experts,))],
         compiler_params=pltpu.CompilerParams(
             collective_id=0, has_side_effects=True, vmem_limit_bytes=56 * 1024 * 1024
@@ -644,7 +739,17 @@
         pool_input,
         pool_weight,
     )
-    return (pool_out, expert_out)
+    return pl.pallas_call(
+        store_kernel,
+        out_shape=(
+            jax.ShapeDtypeStruct(pool_out.shape, bf16),
+            jax.ShapeDtypeStruct(expert_out.shape, bf16),
+        ),
+        in_specs=[vmem, vmem],
+        out_specs=(anywhere, anywhere),
+        scratch_shapes=[dma((2,))],
+        compiler_params=pltpu.CompilerParams(vmem_limit_bytes=1024 * 1024),
+    )(pool_out, expert_out)
 
 
 def solution(mesh):

time: 60.1 us -> 58 us (0.965)
  local copies, waits for them, and re-layouts: 1.38 us -> 0 us
  Pallas kernels: 57.9 us -> 57.2 us
    pallas_call x1, Pallas kernels: 57.9 us -> 56.4 us  [local(): pl.pallas_call(functools.partial(expert_kernel, (experts, ny, nx, slots,...]
    unnamed x2 -> x0, local copies, waits for them, and re-layouts: 1.38 us -> none
    pallas_call x0 -> x1, Pallas kernels: none -> 0.78 us  [local(): pl.pallas_call(store_kernel, out_shape=(jax.ShapeDtypeStruct(pool_out.sha...]
where the time goes in v2:
time: 58 us; the launch traced here: 57.8 us
  Pallas kernels  57.2 us (99%)
  between operations  0.64 us (1%)
    pallas_call x1, Pallas kernels, local(): pl.pallas_call(functools.partial(expert_kernel, (experts, ny, nx, slots,...  56.4 us

profile of v2, /device:TPU:1, one launch (start us, length us, event | category | flops | bytes accessed | tf_op | source)
XLA Modules:
  0.0 57.8 jit_solution(15754489376939138797)
XLA Ops:
  0.6 56.4 %shard_map.122 = (bf16[192,512]{1,0:T(8,128)(2,1)S(1)}, bf16[256,512]{1,0:T(8,128)(2,1)S(1)}) custom-call(s32[2,192]{1,0:T(2,128)} %bitcast.7, f32[2,192]{1,0:T(2,128)} %bitcast.8, f32[1,2048]{1,0:T(1,128)} %bitcast.5, f32[1,2048]{1,0:T(1,128)} %bitcast.6, f32[1,512]{1,0:T(1,128)} %bitcast.9, bf16[192,2048]{1,0:T(8,128)(2,1)} %tokens_hbm.1, ...), custom_call_target="tpu_custom_call" | custom-call | tf_op jit(solution)/shard_map/pallas_call | solution.py:671
  57.1 0.8 %shard_map.123 = (bf16[256,512]{1,0:T(8,128)(2,1)}, bf16[192,512]{1,0:T(8,128)(2,1)}) custom-call(bf16[256,512]{1,0:T(8,128)(2,1)S(1)} %get-tuple-element.4.pool_ref, bf16[192,512]{1,0:T(8,128)(2,1)S(1)} %get-tuple-element.5.expert_ref), custom_call_target="tpu_custom_call" | custom-call | tf_op jit(solution)/shard_map/pallas_call | solution.py:742

commit v3 on v2

--- a/solution.py
+++ b/solution.py
@@ -580,6 +580,8 @@
                 keep_own(0)
                 keep_own(1)
             else:
+                while pending:
+                    pending.pop(0).wait_send()
                 finish_own()
             return
         if core == 0:

time: 58 us -> 57.9 us (level)
  no operation moved by 1% of the time
where the time goes in v3:
time: 57.9 us; the launch traced here: 57.7 us
  Pallas kernels  57.1 us (99%)
  between operations  0.64 us (1%)
    pallas_call x1, Pallas kernels, local(): pl.pallas_call(functools.partial(expert_kernel, (experts, ny, nx, slots,...  56.3 us

profile of v3, /device:TPU:1, one launch (start us, length us, event | category | flops | bytes accessed | tf_op | source)
XLA Modules:
  0.0 57.7 jit_solution(2937790473265979433)
XLA Ops:
  0.6 56.3 %shard_map.122 = (bf16[192,512]{1,0:T(8,128)(2,1)S(1)}, bf16[256,512]{1,0:T(8,128)(2,1)S(1)}) custom-call(s32[2,192]{1,0:T(2,128)} %bitcast.7, f32[2,192]{1,0:T(2,128)} %bitcast.8, f32[1,2048]{1,0:T(1,128)} %bitcast.5, f32[1,2048]{1,0:T(1,128)} %bitcast.6, f32[1,512]{1,0:T(1,128)} %bitcast.9, bf16[192,2048]{1,0:T(8,128)(2,1)} %tokens_hbm.1, ...), custom_call_target="tpu_custom_call" | custom-call | tf_op jit(solution)/shard_map/pallas_call | solution.py:673
  57.0 0.8 %shard_map.123 = (bf16[256,512]{1,0:T(8,128)(2,1)}, bf16[192,512]{1,0:T(8,128)(2,1)}) custom-call(bf16[256,512]{1,0:T(8,128)(2,1)S(1)} %get-tuple-element.4.pool_ref, bf16[192,512]{1,0:T(8,128)(2,1)S(1)} %get-tuple-element.5.expert_ref), custom_call_target="tpu_custom_call" | custom-call | tf_op jit(solution)/shard_map/pallas_call | solution.py:744
